TPU v7x, 32 devices: a whole 2x2x4 slice. The times are simulated.
32 devices in a mesh: fs: 4 (over z), tp: 8 (over y, x, core).
Axes of the slice: x: 2, y: 2, z: 4, core: 2. Of those that a mesh axis runs over, the one named last changes fastest.
Arguments:
- tokens: bfloat16 [1024, 2048], P('fs', 'tp'), may hold values from -6 to 6
- norm_gain: float32 [2048], P('tp'), may hold values from 0.1 to 1.9
- gate_master: float32 [8, 3584, 2048], P(None, 'fs', 'tp'), may hold values from -0.125 to 0.125
- up_master: float32 [8, 3584, 2048], P(None, 'fs', 'tp'), may hold values from -0.125 to 0.125
- down_master: float32 [8, 3584, 2048], P(None, 'fs', 'tp'), may hold values from -0.0625 to 0.0625
- routes: int32 [1024, 2], P('fs'), may hold values from 0 to 3, all different within a row; in each aligned block of 256 rows (0 to 255, 256 to 511, ...) at most 128 rows name the same one
- route_logits: float32 [1024, 2], P('fs'), may hold values from -8 to 8
Outputs:
- gate_serve: bfloat16 [8, 3584, 2048], P('tp', 'fs')
- up_serve: bfloat16 [8, 3584, 2048], P('tp', 'fs')
- down_serve: bfloat16 [8, 3584, 2048], P('tp', 'fs')
- mixed_tokens: bfloat16 [1024, 2048], P('fs', 'tp')
Inputs may be any that keep to these rules, and one draw needn't show every extreme that they name: `routes`: each row names 2 different experts; in every aligned block of 256 rows each expert is named by exactly 128 rows.
All inputs are finite; a program needn't handle non-finite values.
Results may differ from a plain program's by a relative error of at most 0.024.
Values may be sent and summed in bfloat16 or wider, within the bound.
A program may use at most 128 MiB of HBM per device.

v0:
```python
import jax
import jax.numpy as jnp
from jax import lax
from jax.sharding import PartitionSpec as P

epsilon = 1e-05


def partner(value, axis, apart):
    mask = 2**apart
    pairs = [(source, source ^ mask) for source in range(lax.axis_size(axis))]
    return lax.ppermute(value, axis, pairs)


def normalize(row_block):
    widened = row_block.astype(jnp.float32)
    row_scale = lax.rsqrt(jnp.mean(widened * widened, axis=-1, keepdims=True) + epsilon)
    return (widened * row_scale).astype(jnp.bfloat16)


def slab_hidden(inputs, gate_slab, up_slab):
    contract_dims = (((1,), (1,)), ((), ()))
    gate_pre = lax.dot_general(inputs, gate_slab, contract_dims, preferred_element_type=jnp.float32)
    up_pre = lax.dot_general(inputs, up_slab, contract_dims, preferred_element_type=jnp.float32)
    return (jax.nn.silu(gate_pre) * up_pre).astype(jnp.bfloat16)


def in_order(parity, mine, theirs):
    first = jnp.where(parity == 0, mine, theirs)
    second = jnp.where(parity == 0, theirs, mine)
    return (first, second)


def local(tokens, norm_gain, gate_master, up_master, down_master, routes, route_logits):
    tok_rows = tokens.shape[0]
    block_rows = gate_master.shape[1]
    slab_count = lax.axis_size("tp")
    experts = slab_count // 2
    capacity = tok_rows * routes.shape[1] // experts
    half_cap = capacity // 2
    own_expert = lax.axis_index("tp") // 2
    parity = lax.axis_index("tp") % 2
    gain_row = norm_gain[None, None, :]
    gate_ready = (gate_master * gain_row).astype(jnp.bfloat16)
    up_ready = (up_master * gain_row).astype(jnp.bfloat16)
    down_ready = down_master.astype(jnp.bfloat16)
    first_prob = jax.nn.sigmoid(route_logits[:, 0] - route_logits[:, 1])
    choice_prob = jnp.stack([first_prob, 1.0 - first_prob], axis=1)
    expert_ids = jnp.arange(experts, dtype=jnp.int32)
    matches = (routes[:, :, None] == expert_ids[None, None, :]).astype(jnp.float32)
    chosen = jnp.sum(matches, axis=1)
    weight = jnp.sum(matches * choice_prob[:, :, None], axis=1)
    position = jnp.cumsum(chosen, axis=0) - 1.0
    slot_ids = jnp.arange(capacity, dtype=jnp.float32)
    placed = chosen.T[:, None, :] * (position.T[:, None, :] == slot_ids[None, :, None]).astype(
        jnp.float32
    )
    own_pick = lax.dynamic_index_in_dim(placed, own_expert, 0, keepdims=False).astype(jnp.bfloat16)
    combine = (placed * weight.T[:, None, :]).reshape(experts * capacity, tok_rows)
    whole_rows = lax.all_gather(tokens, "tp", axis=1, tiled=True)
    normed = normalize(whole_rows)
    gate_serve, up_serve, down_serve = (
        lax.all_to_all(gate_ready, "tp", split_axis=0, concat_axis=2, tiled=True),
        lax.all_to_all(up_ready, "tp", split_axis=0, concat_axis=2, tiled=True),
        lax.all_to_all(down_ready, "tp", split_axis=0, concat_axis=2, tiled=True),
    )
    picked = jnp.dot(own_pick, normed, preferred_element_type=jnp.float32).astype(jnp.bfloat16)
    hidden_all = slab_hidden(
        lax.all_gather(picked, "fs", axis=0, tiled=True), gate_serve[0], up_serve[0]
    )
    split_rows = hidden_all.reshape(-1, 2, half_cap, block_rows)
    mine = lax.dynamic_index_in_dim(split_rows, parity, 1, keepdims=False)
    outgoing = lax.dynamic_index_in_dim(split_rows, 1 - parity, 1, keepdims=False)
    received, other_down = partner((outgoing, down_serve[0]), "tp", 0)
    first_hidden, second_hidden = in_order(parity, mine, received)
    hidden = jnp.concatenate([first_hidden, second_hidden], axis=-1).reshape(-1, 2 * block_rows)
    first_down, second_down = in_order(parity, down_serve[0], other_down)
    down_pair = jnp.concatenate([first_down, second_down], axis=0)
    expert_out = lax.psum_scatter(
        jnp.dot(hidden, down_pair, preferred_element_type=jnp.float32).astype(jnp.bfloat16),
        "fs",
        scatter_dimension=0,
        tiled=True,
    )
    returned = lax.all_to_all(expert_out, "tp", split_axis=1, concat_axis=0, tiled=True)
    mixed_tokens = jnp.dot(combine.T, returned.astype(jnp.float32), precision=lax.Precision.HIGHEST)
    return (gate_serve, up_serve, down_serve, mixed_tokens.astype(jnp.bfloat16))


def solution(mesh):
    placed = (
        P("fs", "tp"),
        P("tp"),
        P(None, "fs", "tp"),
        P(None, "fs", "tp"),
        P(None, "fs", "tp"),
        P("fs", None),
        P("fs", None),
    )
    return jax.shard_map(
        local,
        mesh=mesh,
        in_specs=placed,
        out_specs=(P("tp", "fs", None), P("tp", "fs", None), P("tp", "fs", None), P("fs", "tp")),
        check_vma=False,
    )
```

profile of v0, /device:TPU:1, one launch (start us, length us, event | category | flops | bytes accessed | tf_op | source)
XLA Modules:
  0.0 258.1 jit_solution(9493894452800540472)
XLA Ops:
  7.2 8.4 %copy.29 = f32[8,896,256]{1,2,0:T(8,128)} copy(f32[8,896,256]{2,1,0:T(8,128)} %param.9) | data formatting | bytes 14680064 | tf_op args[2]
  15.6 8.5 %copy.30 = f32[8,896,256]{1,2,0:T(8,128)} copy(f32[8,896,256]{2,1,0:T(8,128)} %param.10) | data formatting | bytes 14680064 | tf_op args[3]
  24.1 10.0 %multiply_convert_fusion = (bf16[8,896,256]{1,2,0:T(8,128)(2,1)}, bf16[8,896,256]{1,2,0:T(8,128)(2,1)}) fusion(f32[8,896,256]{1,2,0:T(8,128)} %copy.30, f32[256]{0:T(256)S(1)} %copy-done.2, f32[8,896,256]{1,2,0:T(8,128)} %copy.29), kind=kLoop, calls=%fused_computation.4 | loop fusion | flops 7340032 | bytes 22021120 | tf_op jit(solution)/shard_map/convert_element_type | solution.py:45
  34.1 5.2 %all-to-all-start = ((bf16[8,896,256]{1,2,0:T(8,128)(2,1)}), bf16[8,896,256]{1,2,0:T(8,128)(2,1)}, u32[]{:S(2)}, u32[]{:S(2)}) async-start(bf16[8,896,256]{1,2,0:T(8,128)(2,1)} %get-tuple-element.21), calls=%async_computation | async-start | bytes 7340032 | tf_op jit(solution)/shard_map/all_to_all | solution.py:63
  39.3 6.9 %copy.31 = bf16[8,896,256]{1,2,0:T(8,128)(2,1)} copy(f32[8,896,256]{2,1,0:T(8,128)} %param.11) | data formatting | bytes 11010048 | tf_op args[4]
  46.2 33.1 %all-to-all-done = bf16[8,896,256]{1,2,0:T(8,128)(2,1)} async-done(((bf16[8,896,256]{1,2,0:T(8,128)(2,1)}), bf16[8,896,256]{1,2,0:T(8,128)(2,1)}, u32[]{:S(2)}, u32[]{:S(2)}) %all-to-all-start) | async-done | bytes 3670048 | tf_op jit(solution)/shard_map/all_to_all | solution.py:63
  79.3 7.9 %all-to-all-start.2 = ((bf16[8,896,256]{1,2,0:T(8,128)(2,1)}), bf16[8,896,256]{1,2,0:T(8,128)(2,1)}, u32[]{:S(2)}, u32[]{:S(2)}) async-start(bf16[8,896,256]{1,2,0:T(8,128)(2,1)} %copy.31), calls=%async_computation.2 | async-start | bytes 7340032 | tf_op jit(solution)/shard_map/all_to_all | solution.py:65
  89.8 38.4 %all-gather.3.cloned.1.call-done = bf16[256,2048]{1,0:T(8,128)(2,1)} async-done(((bf16[256,256]{1,0:T(8,128)(2,1)}), bf16[256,2048]{1,0:T(8,128)(2,1)}) %all-gather.3.cloned.1.call-update) | async-done | bytes 1048592 | tf_op jit(solution)/shard_map/all_gather | solution.py:60
  128.2 1.5 fusion.7
  129.8 2.4 convolution_convert_fusion
  132.2 7.2 %all-to-all-start.1 = ((bf16[8,896,256]{1,2,0:T(8,128)(2,1)}), bf16[8,896,256]{1,2,0:T(8,128)(2,1)}, u32[]{:S(2)}, u32[]{:S(2)}) async-start(bf16[8,896,256]{1,2,0:T(8,128)(2,1)} %get-tuple-element.20), calls=%async_computation.1 | async-start | bytes 7340032 | tf_op jit(solution)/shard_map/all_to_all | solution.py:64
  139.6 39.1 %all-gather.5.cloned.1.call-done = bf16[512,2048]{1,0:T(8,128)(2,1)} async-done(((bf16[128,2048]{1,0:T(8,128)(2,1)}), bf16[512,2048]{1,0:T(8,128)(2,1)}) %all-gather.5.cloned.1.call-update) | async-done | bytes 2097168 | tf_op jit(solution)/shard_map/all_gather | solution.py:69
  178.7 6.2 %fusion.16 = f32[512,896]{1,0:T(8,128)} fusion(bf16[512,2048]{1,0:T(8,128)(2,1)} %all-gather.5.cloned.1.call-done, bf16[896,2048]{0,1:T(8,128)(2,1)} %bitcast.15), kind=kOutput, calls=%fused_computation.38 | convolution fusion | flops 1879048192 | bytes 7602176 | tf_op jit(solution)/shard_map/dot_general | solution.py:23
  185.0 5.6 %multiply_convert_fusion.2 = bf16[512,896]{1,0:T(8,128)(2,1)S(1)} fusion(f32[512,896]{1,0:T(8,128)} %fusion.16, bf16[512,2048]{1,0:T(8,128)(2,1)} %all-gather.5.cloned.1.call-done, bf16[896,2048]{0,1:T(8,128)(2,1)} %bitcast.17), kind=kOutput, calls=%fused_computation.14 | convolution fusion | flops 1881800704 | bytes 8519680 | tf_op jit(solution)/shard_map/dot_general | solution.py:24
  191.5 1.4 collective-permute-done
  193.1 3.8 %broadcast_select_fusion.1 = (bf16[896,2048]{0,1:T(8,128)(2,1)S(1)}, bf16[896,2048]{0,1:T(8,128)(2,1)S(1)}) fusion(bf16[896,2048]{0,1:T(8,128)(2,1)} %collective-permute-done.1, pred[]{:T(512)S(6)} %eq.48, bf16[8,896,256]{1,2,0:T(8,128)(2,1)} %all-to-all-done.2), kind=kLoop, calls=%fused_computation.7 | loop fusion | flops 3670016 | bytes 14680065 | tf_op jit(solution)/shard_map/jit(_where)/select_n | solution.py:29
  197.0 3.1 %fusion.4 = bf16[256,2048]{1,0:T(8,128)(2,1)} fusion(bf16[256,1792]{1,0:T(8,128)(2,1)S(1)} %bitcast.58, bf16[896,2048]{0,1:T(8,128)(2,1)S(1)} %get-tuple-element.17, bf16[896,2048]{0,1:T(8,128)(2,1)S(1)} %get-tuple-element.16), kind=kOutput, calls=%fused_computation.10 | convolution fusion | flops 1894252544 | bytes 9306112 | tf_op jit(solution)/shard_map/dot_general | solution.py:80
  200.1 25.6 %reduce-scatter.2.cloned.1.call-done = bf16[64,2048]{1,0:T(8,128)(2,1)} async-done(((bf16[256,2048]{1,0:T(8,128)(2,1)}), bf16[64,2048]{1,0:T(8,128)(2,1)}) %reduce-scatter.2.cloned.1.call-update) | async-done | bytes 262160 | tf_op jit(solution)/shard_map/reduce_scatter | solution.py:79
  225.7 1.7 copy.42
  227.4 4.7 %all-to-all-start.3 = ((bf16[64,8,256]{2,0,1:T(8,128)(2,1)}), bf16[64,8,256]{2,0,1:T(8,128)(2,1)S(1)}, u32[]{:S(2)}, u32[]{:S(2)}) async-start(bf16[64,8,256]{2,0,1:T(8,128)(2,1)} %bitcast.54), calls=%async_computation.4 | async-start | bytes 524288 | tf_op jit(solution)/shard_map/all_to_all | solution.py:85
  232.1 6.1 %copy.35 = bf16[1,896,2048]{2,1,0:T(8,128)(2,1)} copy(bf16[1,896,2048]{1,2,0:T(8,128)(2,1)} %bitcast.2) | data formatting | bytes 7340032
  238.2 6.0 %copy.36 = bf16[1,896,2048]{2,1,0:T(8,128)(2,1)} copy(bf16[1,896,2048]{1,2,0:T(8,128)(2,1)} %bitcast.5) | data formatting | bytes 7340032
  244.2 6.0 %copy.37 = bf16[1,896,2048]{2,1,0:T(8,128)(2,1)} copy(bf16[1,896,2048]{1,2,0:T(8,128)(2,1)} %bitcast.8) | data formatting | bytes 7340032
  250.3 1.3 convolution_convert_fusion.1
  (36 shorter events, 4.0 us)
Async XLA Ops:
  15.6 8.5 %copy-start.2 = (f32[256]{0:T(256)S(1)}, f32[256]{0:T(256)}, u32[]{:S(2)}) copy-start(f32[256]{0:T(256)} %param.8) | copy-start | bytes 3076
  34.1 45.3 %all-to-all-start = ((bf16[8,896,256]{1,2,0:T(8,128)(2,1)}), bf16[8,896,256]{1,2,0:T(8,128)(2,1)}, u32[]{:S(2)}, u32[]{:S(2)}) async-start(bf16[8,896,256]{1,2,0:T(8,128)(2,1)} %get-tuple-element.21), calls=%async_computation | async-start | bytes 7340032 | tf_op jit(solution)/shard_map/all_to_all | solution.py:63
  46.2 41.8 %copy-start = (f32[256,2]{0,1:T(2,128)S(1)}, f32[256,2]{0,1:T(2,128)}, u32[]{:S(2)}) copy-start(f32[256,2]{0,1:T(2,128)} %param.13) | copy-start | bytes 6148
  46.2 41.9 %copy-start.1 = (s32[256,2]{0,1:T(2,128)S(1)}, s32[256,2]{0,1:T(2,128)}, u32[]{:S(2)}) copy-start(s32[256,2]{0,1:T(2,128)} %param.12) | copy-start | bytes 6148
  79.3 52.9 %all-to-all-start.2 = ((bf16[8,896,256]{1,2,0:T(8,128)(2,1)}), bf16[8,896,256]{1,2,0:T(8,128)(2,1)}, u32[]{:S(2)}, u32[]{:S(2)}) async-start(bf16[8,896,256]{1,2,0:T(8,128)(2,1)} %copy.31), calls=%async_computation.2 | async-start | bytes 7340032 | tf_op jit(solution)/shard_map/all_to_all | solution.py:65
  87.2 41.0 %all-gather.3.cloned.1.call-start = ((), (), s32[]{:S(2)}) async-start(), calls=%async_computation.5 | async-start | bytes 1179648 | tf_op jit(solution)/shard_map/all_gather | solution.py:60
  87.9 90.8 %all-gather.5.cloned.1.call-start = ((), (), s32[]{:S(2)}) async-start(), calls=%async_computation.6 | async-start | bytes 2621440 | tf_op jit(solution)/shard_map/all_gather | solution.py:69
  132.2 52.7 %all-to-all-start.1 = ((bf16[8,896,256]{1,2,0:T(8,128)(2,1)}), bf16[8,896,256]{1,2,0:T(8,128)(2,1)}, u32[]{:S(2)}, u32[]{:S(2)}) async-start(bf16[8,896,256]{1,2,0:T(8,128)(2,1)} %get-tuple-element.20), calls=%async_computation.1 | async-start | bytes 7340032 | tf_op jit(solution)/shard_map/all_to_all | solution.py:64
  139.4 86.3 %reduce-scatter.2.cloned.1.call-start = ((), (), s32[]{:S(2)}) async-start(), calls=%async_computation.7 | async-start | bytes 1310720 | tf_op jit(solution)/shard_map/reduce_scatter | solution.py:79
  139.4 53.7 %collective-permute-start.1 = (bf16[896,2048]{0,1:T(8,128)(2,1)}, bf16[896,2048]{0,1:T(8,128)(2,1)}, u32[]{:S(2)}, u32[]{:S(2)}) collective-permute-start(bf16[896,2048]{0,1:T(8,128)(2,1)} %bitcast.23), channel_id=1, source_target_pairs={{0,1},{1,0},{2,3},{3,2},{4,5},{5,4},{6,7},{7,6},{8,9},{9,8},{10,11... | collective-permute-start | bytes 11010056 | tf_op jit(solution)/shard_map/ppermute | solution.py:12
  190.6 2.4 collective-permute-start
  227.4 22.9 %all-to-all-start.3 = ((bf16[64,8,256]{2,0,1:T(8,128)(2,1)}), bf16[64,8,256]{2,0,1:T(8,128)(2,1)S(1)}, u32[]{:S(2)}, u32[]{:S(2)}) async-start(bf16[64,8,256]{2,0,1:T(8,128)(2,1)} %bitcast.54), calls=%async_computation.4 | async-start | bytes 524288 | tf_op jit(solution)/shard_map/all_to_all | solution.py:85
Sparse Core Ops, SparseCore 0:
  89.9 38.2 all-gather.2
  132.3 46.3 all-gather.4
  200.2 25.4 reduce-scatter.1
where the time goes:
time: 259 us; the launch traced here: 258 us
  waiting for transfers between devices  138 us (53%)
  local copies, waits for them, and re-layouts  44 us (17%)
  starting transfers between devices  26.2 us (10%)
  matrix products  18.6 us (7%)
  other arithmetic  17 us (7%)
  between operations  13.8 us (5%)
    unnamed x13, local copies, waits for them, and re-layouts  42 us
    all_gather x1, waiting for transfers between devices, local(): lax.all_gather(picked, 'fs', axis=0, tiled=True)  39.1 us
    all_gather x1, waiting for transfers between devices, local(): whole_rows = lax.all_gather(tokens, 'tp', axis=1, tiled=True)  38.4 us
    all_to_all x1, waiting for transfers between devices, local(): lax.all_to_all(gate_ready, 'tp', split_axis=0, concat_axis=2, tiled=True)  33.1 us
    reduce_scatter x1, waiting for transfers between devices, local(): lax.psum_scatter(jnp.dot(hidden, down_pair, preferred_element_type=jnp.fl...  25.6 us
    convert_element_type x1, other arithmetic, local(): up_ready = (up_master * gain_row).astype(jnp.bfloat16)  9.99 us
    all_to_all x1, starting transfers between devices, local(): lax.all_to_all(down_ready, 'tp', split_axis=0, concat_axis=2, tiled=True)  7.9 us
    all_to_all x1, starting transfers between devices, local(): lax.all_to_all(up_ready, 'tp', split_axis=0, concat_axis=2, tiled=True)  7.16 us
  transfers between devices with their start and end apart: 9, of which 5 were waited for; matrix products, arithmetic and copies ran while one was open for 17% of the time, Pallas kernels for 0%

commit v1 on v0

v1 whole, which is shorter than its diff:
```python
import functools

import jax
import jax.numpy as jnp
from jax import lax
from jax.experimental import pallas as pl
from jax.experimental.pallas import tpu as pltpu
from jax.sharding import PartitionSpec as P

epsilon = 1e-05
MESH = pl.DeviceIdType.MESH
NT = (((1,), (1,)), ((), ()))
NN = (((1,), (0,)), ((), ()))
TN = (((0,), (0,)), ((), ()))
SLOTS = 4


def dot(a, b, dims):
    return lax.dot_general(a, b, dims, preferred_element_type=jnp.float32)


def flipped(index, mask):
    result, bit = index, 1
    while bit <= mask:
        if mask & bit:
            result = result + bit * (1 - 2 * ((index // bit) % 2))
        bit *= 2
    return result


def kernel(
    nf, nt, tok_ref, gain_ref, gate_ref, up_ref, down_ref, routes_ref, logits_ref,
    gate_out, up_out, down_out, mixed_ref,
    stage, snd, wv, place, comb_hi, comb_lo, pick, xin, xall, gate_pre, hid, part, pin, psum, zin, ret,
    stage_sem, w_send, w_recv, x_send, x_recv, z_send, z_recv, p_send, p_recv,
    h_send, h_recv, s_send, s_recv, r_send, r_recv, out_sem,
):
    f, me = lax.axis_index("fs"), lax.axis_index("tp")
    parity = me % 2
    partner = me + 1 - 2 * parity
    rows, cols = tok_ref.shape
    block = gate_ref.shape[1]
    half = pick.shape[1]
    cap = 2 * half
    experts = nt // 2
    masters = (gate_ref, up_ref, down_ref)
    outs = (gate_out, up_out, down_out)
    order = list(range(nt - 1, -1, -1))
    jobs = [(w, k) for w in range(3) for k in order]

    def load(i):
        w, k = jobs[i]
        return pltpu.make_async_copy(
            masters[w].at[flipped(me, k)], stage.at[i % SLOTS], stage_sem.at[i % SLOTS]
        )

    def remote(src, dst, send, recv, to_f, to_t):
        return pltpu.make_async_remote_copy(
            src_ref=src, dst_ref=dst, send_sem=send, recv_sem=recv,
            device_id=(to_f, to_t), device_id_type=MESH,
        )

    for i in range(SLOTS):
        load(i).start()
    barrier = pltpu.get_barrier_semaphore()
    for k in range(1, nt):
        pl.semaphore_signal(barrier, inc=1, device_id=(f, flipped(me, k)), device_id_type=MESH)

    @pl.loop(1, nf)
    def _(d):
        pl.semaphore_signal(barrier, inc=1, device_id=((f + d) % nf, me), device_id_type=MESH)

    pl.semaphore_wait(barrier, nt - 1 + nf - 1)

    step = 128 if block % 128 == 0 else block

    def weight_copy(w, k):
        return remote(
            snd.at[w, k - 1], wv.at[w, me], w_send.at[w, k - 1], w_recv.at[w, k - 1], f, flipped(me, k)
        )

    def convert(i):
        w, k = jobs[i]
        slot = i % SLOTS
        load(i).wait()
        gain = gain_ref[...]

        @pl.loop(0, block // step)
        def _(c):
            at = pl.ds(pl.multiple_of(c * step, 16), step)
            value = stage[slot, at, :]
            if w < 2:
                value = value * gain
            value = value.astype(jnp.bfloat16)
            if k:
                snd[w, k - 1, at, :] = value
            else:
                wv[w, me, at, :] = value

        if k:
            weight_copy(w, k).start()
        if i + SLOTS < len(jobs):
            load(i + SLOTS).start()

    def x_copy(k):
        to = flipped(me, k)
        return remote(pick.at[to], xin.at[me], x_send.at[k - 1], x_recv.at[k - 1], f, to)

    def route():
        r0, r1 = routes_ref[0:1, :], routes_ref[1:2, :]
        l0, l1 = logits_ref[0:1, :], logits_ref[1:2, :]
        p0 = 1.0 / (1.0 + jnp.exp(l1 - l0))
        p1 = 1.0 / (1.0 + jnp.exp(l0 - l1))
        padded = -(-experts // 8) * 8
        ids = lax.broadcasted_iota(jnp.int32, (padded, rows), 0)
        first = jnp.where(ids == r0, 1.0, 0.0)
        second = jnp.where(ids == r1, 1.0, 0.0)
        chosen = first + second
        weight = first * p0 + second * p1
        before = lax.broadcasted_iota(jnp.int32, (rows, rows), 0)
        after = lax.broadcasted_iota(jnp.int32, (rows, rows), 1)
        upto = jnp.where(before <= after, 1.0, 0.0).astype(jnp.bfloat16)
        position = dot(chosen.astype(jnp.bfloat16), upto, NN) - 1.0
        slots = lax.broadcasted_iota(jnp.int32, (cap, rows), 0).astype(jnp.float32)
        for e in range(experts):
            hit = jnp.where(slots == position[e : e + 1, :], 1.0, 0.0) * chosen[e : e + 1, :]
            placed = hit.astype(jnp.bfloat16)
            scaled = hit * weight[e : e + 1, :]
            high = scaled.astype(jnp.bfloat16)
            at = pl.ds(e * cap, cap)
            comb_hi[at, :] = high
            comb_lo[at, :] = (scaled - high.astype(jnp.float32)).astype(jnp.bfloat16)
            got = dot(placed, tok_ref[...], NN).astype(jnp.bfloat16)
            pick[2 * e] = got[:half]
            pick[2 * e + 1] = got[half:]
        xin[me] = pick[me]
        for k in order[:-1]:
            x_copy(k).start()

    early = 2
    for i in range(early):
        convert(i)
    route()
    for i in range(early, len(jobs)):
        convert(i)

    for k in order[:-1]:
        x_copy(k).wait_recv()
    total = jnp.zeros((half, 1), jnp.float32)
    for s in range(nt):
        v = xin[s].astype(jnp.float32)
        total = total + jnp.sum(v * v, axis=-1, keepdims=True)
    scale = lax.rsqrt(total / (nt * cols) + epsilon)

    def rows_of(p, g):
        return pl.ds(pl.multiple_of((p * nf + g) * half, 16), half)

    mine = rows_of(parity, f)
    for s in range(nt):
        xall[s, mine, :] = (xin[s].astype(jnp.float32) * scale).astype(jnp.bfloat16)

    def z_copy(d):
        here = xall.at[:, mine, :]
        return remote(here, here, z_send.at[d], z_recv.at[d], (f + d) % nf, me)

    def p_copy(d):
        here = xall.at[:, rows_of(parity, (f + nf - d) % nf), :]
        return remote(here, here, p_send.at[d], p_recv.at[d], f, partner)

    p_copy(0).start()

    @pl.loop(1, nf)
    def _(d):
        z_copy(d).start()

    @pl.loop(1, nf)
    def _(d):
        here = xall.at[:, rows_of(parity, (f + nf - d) % nf), :]
        remote(here, here, z_send.at[d], z_recv.at[d], (f + d) % nf, me).wait_recv()
        p_copy(d).start()

    @pl.loop(0, nf)
    def _(d):
        here = xall.at[:, rows_of(1 - parity, (f + nf - d) % nf), :]
        remote(here, here, p_send.at[d], p_recv.at[d], f, partner).wait_recv()

    def out_copy(w, k):
        s = flipped(me, k)
        to = outs[w].at[0, :, pl.ds(pl.multiple_of(s * cols, 128), cols)]
        return pltpu.make_async_copy(wv.at[w, s], to, out_sem.at[w, k])

    def arrived(w, k):
        if k:
            s = flipped(me, k)
            remote(
                snd.at[w, k - 1], wv.at[w, s], w_send.at[w, k - 1], w_recv.at[w, k - 1], f, s
            ).wait_recv()
        out_copy(w, k).start()

    def product(w, at):
        acc = dot(xall[0], wv[w, 0, at, :], NT)
        for s in range(1, nt):
            acc = acc + dot(xall[s], wv[w, s, at, :], NT)
        return acc

    def tile(c):
        return pl.ds(pl.multiple_of(c * step, 16), step)

    def lanes(c):
        return pl.ds(pl.multiple_of(c * step, 128), step) if block % 128 == 0 else slice(None)

    for k in order:
        arrived(0, k)

    @pl.loop(0, block // step)
    def _(c):
        gate_pre[:, lanes(c)] = product(0, tile(c))

    for k in order:
        arrived(1, k)

    @pl.loop(0, block // step)
    def _(c):
        gate = gate_pre[:, lanes(c)]
        hid[:, lanes(c)] = (gate / (1.0 + jnp.exp(-gate)) * product(1, tile(c))).astype(jnp.bfloat16)

    side = nf * half

    def pair_at(g):
        return flipped(me // 2, nt // 2 - 1 - g)

    def side_rows(p):
        return pl.ds(pl.multiple_of(p * side, 16), side)

    def h_copy(g):
        q = pair_at(g)
        return remote(
            part.at[q, :, side_rows(1 - parity), :], pin.at[q], h_send.at[g], h_recv.at[g], f, partner
        )

    def s_copy(g, d):
        q, to = pair_at(g), (f + d) % nf
        return remote(psum.at[q, to], zin.at[g, d], s_send.at[g, d], s_recv.at[g, d], to, me)

    def r_copy(k):
        s = flipped(me, k)
        return remote(
            psum.at[s // 2, f, s % 2], ret.at[pl.ds(pl.multiple_of(me * half, 16), half), :],
            r_send.at[k - 1], r_recv.at[k - 1], f, s,
        )

    def stage_a(g):
        ks = (nt - 1 - 2 * g, nt - 2 - 2 * g)
        for k in ks:
            arrived(2, k)
        q = pair_at(g)
        for o in range(2):
            part[q, o] = dot(hid[...], wv[2, 2 * q + o], NN).astype(jnp.bfloat16)
        h_copy(g).start()

    def stage_b(g):
        q = pair_at(g)
        h_copy(g).wait_recv()
        for o in range(2):
            both = part[q, o, side_rows(parity), :].astype(jnp.float32) + pin[q, o].astype(jnp.float32)
            both = both.astype(jnp.bfloat16)
            for j in range(nf):
                psum[q, j, o] = both[j * half : (j + 1) * half]

        @pl.loop(1, nf)
        def _(d):
            s_copy(g, d).start()

    def stage_c(g):
        q = pair_at(g)

        @pl.loop(1, nf)
        def _(d):
            s_copy(g, d).wait_recv()

        for o in range(2):
            acc = psum[q, f, o].astype(jnp.float32)
            for d in range(1, nf):
                acc = acc + zin[g, d, o].astype(jnp.float32)
            psum[q, f, o] = acc.astype(jnp.bfloat16)
        for k in (nt - 1 - 2 * g, nt - 2 - 2 * g):
            if k:
                r_copy(k).start()
            else:
                ret[pl.ds(pl.multiple_of(me * half, 16), half), :] = psum[me // 2, f, me % 2]

    pairs = nt // 2
    for g in range(pairs):
        stage_a(g)
        stage_b(g)
        if g:
            stage_c(g - 1)
    stage_c(pairs - 1)
    for k in order[:-1]:
        r_copy(k).wait_recv()
    mixed = dot(comb_hi[...], ret[...], TN) + dot(comb_lo[...], ret[...], TN)
    mixed_ref[...] = mixed.astype(jnp.bfloat16)

    for k in order:
        for w in range(3):
            out_copy(w, k).wait()
            if k:
                weight_copy(w, k).wait_send()
        if k:
            x_copy(k).wait_send()
            r_copy(k).wait_send()
    p_copy(0).wait_send()

    @pl.loop(1, nf)
    def _(d):
        z_copy(d).wait_send()
        p_copy(d).wait_send()
        for g in range(pairs):
            s_copy(g, d).wait_send()

    for g in range(pairs):
        h_copy(g).wait_send()


def local(tokens, norm_gain, gate_master, up_master, down_master, routes, route_logits):
    nf, nt = lax.axis_size("fs"), lax.axis_size("tp")
    rows, cols = tokens.shape
    block = gate_master.shape[1]
    half = rows * routes.shape[1] // nt
    every = 2 * nf * half
    pairs = nt // 2
    bf16 = jnp.bfloat16
    served = jax.ShapeDtypeStruct((1, block, nt * cols), bf16)
    hbm = pl.BlockSpec(memory_space=pl.ANY)
    vmem = pl.BlockSpec(memory_space=pltpu.VMEM)
    dma = pltpu.SemaphoreType.DMA
    return pl.pallas_call(
        functools.partial(kernel, nf, nt),
        out_shape=(served, served, served, jax.ShapeDtypeStruct((rows, cols), bf16)),
        in_specs=[vmem, vmem, hbm, hbm, hbm, vmem, vmem],
        out_specs=(hbm, hbm, hbm, vmem),
        scratch_shapes=[
            pltpu.VMEM((SLOTS, block, cols), jnp.float32),
            pltpu.VMEM((3, nt - 1, block, cols), bf16),
            pltpu.VMEM((3, nt, block, cols), bf16),
            pltpu.VMEM((16, 128), bf16),
            pltpu.VMEM((nt * half, rows), bf16),
            pltpu.VMEM((nt * half, rows), bf16),
            pltpu.VMEM((nt, half, cols), bf16),
            pltpu.VMEM((nt, half, cols), bf16),
            pltpu.VMEM((nt, every, cols), bf16),
            pltpu.VMEM((every, block), jnp.float32),
            pltpu.VMEM((every, block), bf16),
            pltpu.VMEM((pairs, 2, every, cols), bf16),
            pltpu.VMEM((pairs, 2, every // 2, cols), bf16),
            pltpu.VMEM((pairs, nf, 2, half, cols), bf16),
            pltpu.VMEM((pairs, nf, 2, half, cols), bf16),
            pltpu.VMEM((nt * half, cols), bf16),
            dma((SLOTS,)),
            dma((3, nt - 1)), dma((3, nt - 1)),
            dma((nt - 1,)), dma((nt - 1,)),
            dma((nf,)), dma((nf,)),
            dma((nf,)), dma((nf,)),
            dma((pairs,)), dma((pairs,)),
            dma((pairs, nf)), dma((pairs, nf)),
            dma((nt - 1,)), dma((nt - 1,)),
            dma((3, nt)),
        ],
        compiler_params=pltpu.CompilerParams(
            collective_id=0, has_side_effects=True, vmem_limit_bytes=62 * 1024 * 1024
        ),
    )(tokens, norm_gain.reshape(1, cols), gate_master, up_master, down_master, routes.T, route_logits.T)


def solution(mesh):
    placed = (
        P("fs", "tp"),
        P("tp"),
        P(None, "fs", "tp"),
        P(None, "fs", "tp"),
        P(None, "fs", "tp"),
        P("fs", None),
        P("fs", None),
    )
    return jax.shard_map(
        local,
        mesh=mesh,
        in_specs=placed,
        out_specs=(P("tp", "fs", None), P("tp", "fs", None), P("tp", "fs", None), P("fs", "tp")),
        check_vma=False,
    )
```

time: 259 us -> 164 us (0.63)
  Pallas kernels: 0 us -> 153 us
  waiting for transfers between devices: 138 us -> 0 us
  local copies, waits for them, and re-layouts: 44 us -> 10.4 us
  starting transfers between devices: 26.2 us -> 0 us
  matrix products: 18.6 us -> 0 us
  other arithmetic: 17 us -> 0 us
  between operations: 13.8 us -> 0.65 us
    pallas_call x0 -> x1, Pallas kernels: none -> 153 us  [local(): pl.pallas_call(functools.partial(kernel, nf, nt), out_shape=(served, serv...]
    all_gather x2 -> x0, waiting for transfers between devices: 77.5 us -> none  [the longest x1 39.1 us: local(): lax.all_gather(picked, 'fs', axis=0, tiled=True)]
    all_to_all x4 -> x0, waiting for transfers between devices: 33.1 us -> none  [the longest x1 33.1 us: local(): lax.all_to_all(gate_ready, 'tp', split_axis=0, concat_axis=2, tiled=True)]
    unnamed x13 -> x10, local copies, waits for them, and re-layouts: 42 us -> 10.4 us
    reduce_scatter x1 -> x0, waiting for transfers between devices: 25.6 us -> none  [local(): lax.psum_scatter(jnp.dot(hidden, down_pair, preferred_element_type=jnp.fl...]
    all_to_all x4 -> x0, starting transfers between devices: 25 us -> none  [the longest x1 7.9 us: local(): lax.all_to_all(down_ready, 'tp', split_axis=0, concat_axis=2, tiled=True)]
    dot_general x5 -> x0, matrix products: 18.6 us -> none  [the longest x1 6.23 us: slab_hidden(): lax.dot_general(inputs, gate_slab, contract_dims, preferred_element_type=...]
    convert_element_type x1 -> x0, other arithmetic: 9.99 us -> none  [local(): up_ready = (up_master * gain_row).astype(jnp.bfloat16)]
  transfers between devices with their start and end apart: 9 -> 0, of which waited for: 5 -> 0; matrix products, arithmetic and copies ran while one was open for 17% -> 0% of each run, Pallas kernels for 0% -> 0%
where the time goes in v1:
time: 164 us
  Pallas kernels  153 us (93%)
  local copies, waits for them, and re-layouts  10.4 us (6%)
    pallas_call x1, Pallas kernels, local(): pl.pallas_call(functools.partial(kernel, nf, nt), out_shape=(served, serv...  153 us
    unnamed x10, local copies, waits for them, and re-layouts  10.4 us

profile of v1, /device:TPU:1, one launch (start us, length us, event | category | flops | bytes accessed | tf_op | source)
XLA Modules:
  0.0 163.6 jit_solution(10721640067099594306)
XLA Ops:
  0.6 152.6 %shard_map.102 = (bf16[1,896,2048]{2,1,0:T(8,128)(2,1)}, bf16[1,896,2048]{2,1,0:T(8,128)(2,1)}, bf16[1,896,2048]{2,1,0:T(8,128)(2,1)}, bf16[256,256]{1,0:T(8,128)(2,1)}) custom-call(bf16[256,256]{1,0:T(8,128)(2,1)} %tok_ref.1, f32[1,256]{1,0:T(1,128)} %bitcast.5, f32[8,896,256]{2,1,0:T(8,128)} %gate_ref.1, f32[8,896,256]{2,1,0:T(8,128)} %up_ref.1, ...), custom_call_target="tpu_custom_call" | custom-call | tf_op jit(solution)/shard_map/pallas_call | solution.py:337
  153.2 0.0 copy-start.1
  153.2 4.5 %copy.15 = bf16[1,896,2048]{2,1,0:T(8,128)(2,1)} copy(bf16[1,896,2048]{2,1,0:T(8,128)(2,1)} %get-tuple-element.8) | data formatting | bytes 7340032
  157.7 0.0 copy-done.1
  157.7 0.0 copy-start
  157.7 1.9 %copy.16 = bf16[1,896,2048]{2,1,0:T(8,128)(2,1)} copy(bf16[1,896,2048]{2,1,0:T(8,128)(2,1)S(1)} %copy-done.1) | data formatting | bytes 7340032
  159.6 1.5 copy-done
  161.1 0.0 copy-start.2
  161.1 1.8 %copy.17 = bf16[1,896,2048]{2,1,0:T(8,128)(2,1)} copy(bf16[1,896,2048]{2,1,0:T(8,128)(2,1)S(1)} %copy-done) | data formatting | bytes 7340032
  162.9 0.0 copy-done.2
  162.9 0.7 copy.18
Async XLA Ops:
  153.2 4.5 %copy-start.1 = (bf16[1,896,2048]{2,1,0:T(8,128)(2,1)S(1)}, bf16[1,896,2048]{2,1,0:T(8,128)(2,1)}, u32[]{:S(2)}) copy-start(bf16[1,896,2048]{2,1,0:T(8,128)(2,1)} %get-tuple-element.9) | copy-start | bytes 11010052
  157.7 3.4 %copy-start = (bf16[1,896,2048]{2,1,0:T(8,128)(2,1)S(1)}, bf16[1,896,2048]{2,1,0:T(8,128)(2,1)}, u32[]{:S(2)}) copy-start(bf16[1,896,2048]{2,1,0:T(8,128)(2,1)} %get-tuple-element.10) | copy-start | bytes 11010052
  161.1 1.8 %copy-start.2 = (bf16[256,256]{1,0:T(8,128)(2,1)S(1)}, bf16[256,256]{1,0:T(8,128)(2,1)}, u32[]{:S(2)}) copy-start(bf16[256,256]{1,0:T(8,128)(2,1)} %get-tuple-element.11) | copy-start | bytes 393220
